TPU v7x, 32 devices: a whole 2x2x4 slice. The times are simulated.
32 devices in a mesh: sp: 4 (over z), fs: 4 (over y, x), tp: 2 (over core).
Axes of the slice: x: 2, y: 2, z: 4, core: 2. Of those that a mesh axis runs over, the one named last changes fastest.
Arguments:
- tokens: bfloat16 [16384, 2048], P(('fs', 'sp', 'tp')), parts along dimension 0, may hold values from -6 to 6
- norm_gain: float32 [2048], replicated, may hold values from 0.1 to 1.9
- w_pool: bfloat16 [2048, 1024], P(None, 'tp'), may hold values from -0.125 to 0.125
- w_query: bfloat16 [2048, 1024], P(None, 'tp'), may hold values from -0.125 to 0.125
- w_key: bfloat16 [2048, 1024], P(None, 'tp'), may hold values from -0.125 to 0.125
- w_value: bfloat16 [2048, 1024], P(None, 'tp'), may hold values from -0.125 to 0.125
- w_gate: bfloat16 [2048, 1024], P(None, 'tp'), may hold values from -0.125 to 0.125
- pool_mix: bfloat16 [4, 256, 256], P('tp'), may hold values from -0.375 to 0.375
- pool_bias: float32 [4, 256], P('tp'), may hold values from -3 to 3
- pool_gain: float32 [1024], P('tp'), may hold values from 0.1 to 1.9
- ret_gain: float32 [1024], P('tp'), may hold values from 0.1 to 1.9
- w_out_pool: bfloat16 [1024, 2048], P('tp'), may hold values from -0.125 to 0.125
- w_out_ret: bfloat16 [1024, 2048], P('tp'), may hold values from -0.125 to 0.125
Outputs:
- mixed: bfloat16 [16384, 2048], P(('fs', 'sp', 'tp')), parts along dimension 0
There are 4 independent parts, one for each index of `fs`. A program takes and returns all parts, laid end to end along the dimension named above; an argument that names none is the same for every part. Nothing has to cross between parts.
All inputs are finite; a program needn't handle non-finite values.
Results may differ from a plain program's by a relative error of at most 0.012.
Values may be sent and summed in bfloat16 or wider, within the bound.
A program may use at most 128 MiB of HBM per device.

v0:
```python
import functools
import math

import jax
import jax.numpy as jnp
from jax import lax
from jax.experimental import pallas as pl
from jax.experimental.pallas import tpu as pltpu
from jax.sharding import PartitionSpec as P

GROUP_DIM = 256
HEAD_DIM = 128
CHUNK = 256
SUB = 128
RIM = 16
HOP = 2
PARTS = 4
F32 = jnp.float32
BF16 = jnp.bfloat16


def dot(a, b):
    return jnp.dot(a, b, preferred_element_type=F32)


def layer_kernel(
    n_sp,
    n_tp,
    tokens,
    norm_gain,
    w_pool,
    w_query,
    w_key,
    w_value,
    w_gate,
    pool_mix,
    pool_bias,
    pool_gain,
    ret_gain,
    w_out_pool,
    w_out_ret,
    out_own,
    part_recv,
    tok,
    wts,
    pk,
    pv,
    pp,
    pq,
    pg,
    wo,
    kr,
    qr,
    raw,
    pool_out,
    ret_a,
    ret_b,
    cosine,
    sine,
    decay,
    qdec,
    kdec,
    states,
    total,
    sin_buf,
    sout_buf,
    band,
    ldec,
    part_send,
    tok_sem,
    w_sem,
    wo_sem,
    tok_ss,
    tok_rs,
    st_send,
    st_recv,
    rim_rs,
    part_ss,
    part_rs,
):
    tp = lax.axis_index("tp")
    sp = lax.axis_index("sp")
    rows = tokens.shape[0]
    length = rows * n_tp
    width = w_query.shape[1]
    wide = wo.shape[1]
    heads = width // HEAD_DIM
    groups = w_pool.shape[1] // GROUP_DIM
    chunks = length // CHUNK
    seq_len = length * n_sp
    own = pl.multiple_of(tp * rows, rows)
    other = pl.multiple_of((n_tp - 1 - tp) * rows, rows)
    peer = {"tp": n_tp - 1 - tp}

    tok_in = pltpu.make_async_copy(tokens, tok.at[pl.ds(own, rows)], tok_sem)
    tok_in.start()
    w_in = [
        pltpu.make_async_copy(w, wts.at[i], w_sem.at[i])
        for i, w in enumerate((w_key, w_value, w_pool, w_query, w_gate))
    ]
    w_in[0].start()
    w_in[1].start()
    half = w_out_pool.shape[0]
    wo_in = [
        pltpu.make_async_copy(w_out_pool, wo.at[pl.ds(0, half)], wo_sem.at[0]),
        pltpu.make_async_copy(w_out_ret, wo.at[pl.ds(half, width)], wo_sem.at[1]),
    ]

    barrier = pltpu.get_barrier_semaphore()
    pl.semaphore_signal(barrier, inc=1, device_id=peer, device_id_type=pl.DeviceIdType.MESH)

    @pl.when(sp > 0)
    def _():
        pl.semaphore_signal(
            barrier, inc=1, device_id={"sp": sp - 1}, device_id_type=pl.DeviceIdType.MESH
        )

    @pl.when(sp < n_sp - 1)
    def _():
        pl.semaphore_signal(
            barrier, inc=1, device_id={"sp": sp + 1}, device_id_type=pl.DeviceIdType.MESH
        )

    def log_decay(h):
        total_heads = heads * n_tp
        value = jnp.float32(0.0)
        for t in range(n_tp):
            one = -(2.0**-5) * (seq_len / 16.0) ** (-2.0 * (t * heads + h) / (total_heads - 1))
            value = jnp.where(tp == t, jnp.float32(one), value)
        return value

    logs = [log_decay(h) for h in range(heads)]
    lane = lax.broadcasted_iota(jnp.int32, (SUB, HEAD_DIM), 1)
    row = lax.broadcasted_iota(jnp.int32, (SUB, HEAD_DIM), 0)
    hd = HEAD_DIM // 2
    low = lane < hd
    freq = jnp.exp(
        jnp.where(low, lane, lane - hd).astype(F32) * (-math.log(10000.0) / hd)
    )
    ang = row.astype(F32) * freq
    cos_r, sin_r = jnp.cos(ang), jnp.sin(ang)
    subs = length // SUB
    base_row = lax.broadcasted_iota(jnp.int32, (subs, HEAD_DIM), 0)
    base = (sp * length + base_row * SUB).astype(F32) * freq[:subs]
    cos_b, sin_b = jnp.cos(base), jnp.sin(base)
    for b in range(subs):
        cb, sb = cos_b[b : b + 1], sin_b[b : b + 1]
        cosine[b * SUB : (b + 1) * SUB] = cb * cos_r - sb * sin_r
        s = sb * cos_r + cb * sin_r
        sine[b * SUB : (b + 1) * SUB] = jnp.where(low, -s, s)

    step_i = lax.broadcasted_iota(jnp.int32, (CHUNK, HEAD_DIM), 0).astype(F32)
    di = lax.broadcasted_iota(jnp.int32, (CHUNK, CHUNK), 0) - lax.broadcasted_iota(
        jnp.int32, (CHUNK, CHUNK), 1
    )
    dpos = jnp.maximum(di, 0).astype(F32)
    for h in range(heads):
        decay[h] = jnp.where(di >= 0, jnp.exp(logs[h] * dpos), 0.0)
        qdec[h] = jnp.exp(logs[h] * (step_i + 1.0))
        kdec[h] = jnp.exp(logs[h] * (CHUNK - 1.0 - step_i))
    bi = lax.broadcasted_iota(jnp.int32, (SUB, SUB + RIM), 0)
    bj = lax.broadcasted_iota(jnp.int32, (SUB, SUB + RIM), 1)
    back = bi + RIM - bj
    windows = [jnp.left_shift(jnp.int32(2), tp * groups + g) for g in range(groups)]
    for g in range(groups):
        band[g] = jnp.where((back >= 0) & (back < windows[g]), 1.0, 0.0).astype(BF16)

    @pl.when(sp == 0)
    def _():
        pp[0:RIM] = jnp.zeros((RIM, width), BF16)
        sin_buf[...] = jnp.zeros_like(sin_buf)

    neighbours = jnp.where(sp > 0, 1, 0) + jnp.where(sp < n_sp - 1, 1, 0)
    pl.semaphore_wait(barrier, 1 + neighbours)

    part = rows // PARTS

    def tok_copy(i):
        at = pl.ds(pl.multiple_of(own + i * part, part), part)
        return pltpu.make_async_remote_copy(
            src_ref=tok.at[at],
            dst_ref=tok.at[at],
            send_sem=tok_ss.at[i],
            recv_sem=tok_rs.at[i],
            device_id=peer,
            device_id_type=pl.DeviceIdType.MESH,
        )

    def norm_rows(start):
        step = 16

        def body(i, carry):
            at = pl.ds(pl.multiple_of(start + i * step, step), step)
            x = tok[at, :].astype(F32)
            scale = lax.rsqrt(jnp.mean(x * x, axis=-1, keepdims=True) + 1e-06)
            tok[at, :] = (x * scale * norm_gain[...]).astype(BF16)
            return carry

        lax.fori_loop(0, part // step, body, 0, unroll=4)

    def project(w, dst, start, pad=0):
        start = pl.multiple_of(start, CHUNK)
        res = dot(tok[pl.ds(start, CHUNK), :], wts[w])
        dst[pl.ds(pl.multiple_of(start + pad, RIM), CHUNK)] = res.astype(BF16)

    per_half = rows // CHUNK

    def kv_half(start):
        def body(i, carry):
            project(0, pk, start + i * CHUNK)
            project(1, pv, start + i * CHUNK)
            return carry

        lax.fori_loop(0, per_half, body, 0)

    tok_in.wait()
    for copy in w_in[2:] + wo_in:
        copy.start()
    for i in range(PARTS):
        norm_rows(own + i * part)
        if i > 0:
            tok_copy(i - 1).start()
    w_in[0].wait()
    w_in[1].wait()
    tok_copy(PARTS - 1).start()
    kv_half(own)
    for i in range(PARTS):
        tok_copy(i).wait_recv()
    kv_half(other)

    def rotate(x, at):
        return x * cosine[at] + pltpu.roll(x, HEAD_DIM // 2, 1) * sine[at]

    for h in range(heads):
        total[h] = jnp.zeros((HEAD_DIM, HEAD_DIM), F32)
    block_decays = [jnp.exp(jnp.full((1, HEAD_DIM), logs[h] * CHUNK, F32)) for h in range(heads)]
    for h in range(heads):
        ldec[h] = jnp.exp(jnp.full((8, HEAD_DIM), logs[h] * length, F32))

    def state_body(b, carry):
        at = pl.ds(pl.multiple_of(b * CHUNK, CHUNK), CHUNK)
        for h in range(heads):
            cols = slice(h * HEAD_DIM, (h + 1) * HEAD_DIM)
            k = rotate(pk[at, cols].astype(F32), at) * HEAD_DIM**-0.5
            kr[at, cols] = k.astype(BF16)
            kd = (k * kdec[h]).astype(BF16)
            new = lax.dot_general(
                kd, pv[at, cols], (((0,), (0,)), ((), ())), preferred_element_type=F32
            )
            states[b, h] = total[h]
            total[h] = total[h] * block_decays[h] + new
        return carry

    lax.fori_loop(0, chunks, state_body, 0)
    for copy in w_in[2:]:
        copy.wait()

    slots = 3 * chunks

    def st_copy(h):
        return pltpu.make_async_remote_copy(
            src_ref=sout_buf.at[h],
            dst_ref=sin_buf.at[h],
            send_sem=st_send.at[h],
            recv_sem=st_recv.at[h],
            device_id={"sp": sp + 1},
            device_id_type=pl.DeviceIdType.MESH,
        )

    rim_copy = pltpu.make_async_remote_copy(
        src_ref=pp.at[pl.ds(length, RIM)],
        dst_ref=pp.at[pl.ds(0, RIM)],
        send_sem=rim_rs.at[0],
        recv_sem=rim_rs.at[1],
        device_id={"sp": sp + 1},
        device_id_type=pl.DeviceIdType.MESH,
    )

    def relay_head(h):
        @pl.when(sp > 0)
        def _():
            st_copy(h).wait_recv()

        @pl.when(sp < n_sp - 1)
        def _():
            sout_buf[h] = (total[h] + ldec[h, 0:1] * sin_buf[h].astype(F32)).astype(BF16)
            st_copy(h).start()

    def relay(c):
        h = c - HOP * sp

        @pl.when((h >= 0) & (h < heads) & (sp > 0) & (sp < n_sp - 1))
        def _():
            relay_head(h)

    @pl.when(sp == 0)
    def _():
        for h in range(heads):
            relay_head(h)

    def pool_body(c, carry):
        relay(c)
        project(2, pp, c * CHUNK, RIM)
        return carry

    lax.fori_loop(0, chunks, pool_body, 0)

    def query_body(c, carry):
        relay(chunks + c)

        @pl.when((c == 1) & (sp < n_sp - 1))
        def _():
            rim_copy.start()

        project(3, pq, c * CHUNK)
        return carry

    lax.fori_loop(0, chunks, query_body, 0)

    @pl.when(sp > 0)
    def _():
        rim_copy.wait_recv()

    def local_body(b, carry):
        relay(2 * chunks + b)
        project(4, pg, b * CHUNK)
        at = pl.ds(pl.multiple_of(b * CHUNK, CHUNK), CHUNK)
        for h in range(heads):
            cols = slice(h * HEAD_DIM, (h + 1) * HEAD_DIM)
            q = rotate(pq[at, cols].astype(F32), at).astype(BF16)
            qr[at, cols] = q
            scores = lax.dot_general(
                q, kr[at, cols], (((1,), (1,)), ((), ())), preferred_element_type=F32
            )
            scores = (scores * decay[h]).astype(BF16)
            raw[at, cols] = dot(scores, pv[at, cols]) + qdec[h] * dot(
                q, states[b, h].astype(BF16)
            )
        for s in range(CHUNK // SUB):
            first = b * CHUNK + s * SUB
            here = sp * length + first + lax.broadcasted_iota(jnp.int32, (SUB, GROUP_DIM), 0)
            for g in range(groups):
                cols = slice(g * GROUP_DIM, (g + 1) * GROUP_DIM)
                span = pp[pl.ds(pl.multiple_of(first, SUB), SUB + RIM), cols]
                x = pp[pl.ds(pl.multiple_of(first + RIM, RIM), SUB), cols].astype(F32)
                count = jnp.minimum(here + 1, windows[g]).astype(F32)
                diff = (dot(band[g], span) / count - x).astype(BF16)
                mixed = dot(diff, pool_mix[g]) + pool_bias[g : g + 1]
                pool_out[pl.ds(pl.multiple_of(first, SUB), SUB), cols] = (
                    mixed * pool_gain[:, cols]
                ).astype(BF16)
        return carry

    lax.fori_loop(0, chunks, local_body, 0)

    def rest(h, carry):
        late = (h + HOP * sp >= slots) | (sp == n_sp - 1)

        @pl.when(late & (sp > 0))
        def _():
            relay_head(h)

        return carry

    lax.fori_loop(0, heads, rest, 0)
    for copy in wo_in:
        copy.wait()

    def finish(start, ret):
        at = pl.ds(pl.multiple_of(start, CHUNK), CHUNK)
        for h in range(heads):
            cols = slice(h * HEAD_DIM, (h + 1) * HEAD_DIM)
            ahead = jnp.exp(jnp.full((1, HEAD_DIM), logs[h], F32) * start.astype(F32))
            state = (sin_buf[h].astype(F32) * ahead).astype(BF16)
            r = raw[at, cols] + qdec[h] * dot(qr[at, cols], state)
            r = r - jnp.mean(r, axis=-1, keepdims=True)
            var = jnp.mean(r * r, axis=-1, keepdims=True)
            gate = pg[at, cols].astype(F32)
            gated = gate * (1.0 / (1.0 + jnp.exp(-gate))) * ret_gain[:, cols]
            ret[:, cols] = (
                gated * (r * lax.rsqrt(var + 1e-06))
            ).astype(BF16)

    def part_copy(j):
        at = pl.ds(pl.multiple_of(j * CHUNK, CHUNK), CHUNK)
        return pltpu.make_async_remote_copy(
            src_ref=part_send.at[at],
            dst_ref=part_recv.at[at],
            send_sem=part_ss.at[j],
            recv_sem=part_rs.at[j],
            device_id=peer,
            device_id_type=pl.DeviceIdType.MESH,
        )

    tile = 512

    def multiply(start, ret, dst, j):
        at = pl.ds(pl.multiple_of(start, CHUNK), CHUNK)
        mine = slice(j * CHUNK, (j + 1) * CHUNK)
        left = jnp.concatenate([pool_out[at, :], ret[...]], axis=1)
        for n in range(wide // tile):
            cols = slice(n * tile, (n + 1) * tile)
            dst[mine, cols] = dot(left, wo[:, cols]).astype(BF16)

    starts = [other + j * CHUNK for j in range(per_half)] + [
        own + j * CHUNK for j in range(per_half)
    ]
    rets = (ret_a, ret_b)
    finish(starts[0], ret_a)
    for i, start in enumerate(starts):
        sending = i < per_half
        multiply(start, rets[i % 2], part_send if sending else out_own, i % per_half)
        if i + 1 < len(starts):
            finish(starts[i + 1], rets[(i + 1) % 2])
        if sending:
            part_copy(i).start()

    for j in range(per_half):
        part_copy(j).wait_recv()

    for i in range(PARTS):
        tok_copy(i).wait_send()
    for j in range(per_half):
        part_copy(j).wait_send()

    @pl.when(sp < n_sp - 1)
    def _():
        rim_copy.wait_send()
        for h in range(heads):
            st_copy(h).wait_send()


def per_device(
    tokens,
    norm_gain,
    w_pool,
    w_query,
    w_key,
    w_value,
    w_gate,
    pool_mix,
    pool_bias,
    pool_gain,
    ret_gain,
    w_out_pool,
    w_out_ret,
):
    n_sp, n_tp = lax.axis_size("sp"), lax.axis_size("tp")
    rows, model = tokens.shape
    length = rows * n_tp
    width = w_query.shape[1]
    heads = width // HEAD_DIM
    pool_width = w_pool.shape[1]
    groups = pool_width // GROUP_DIM
    chunks = length // CHUNK
    per_half = rows // CHUNK
    wide = w_out_pool.shape[1]
    hbm = pl.BlockSpec(memory_space=pltpu.HBM)
    vmem = pl.BlockSpec(memory_space=pltpu.VMEM)
    dma = pltpu.SemaphoreType.DMA
    flops = 2 * length * model * (pool_width + 4 * width) + 2 * length * (pool_width + width) * wide
    own, received = pl.pallas_call(
        functools.partial(layer_kernel, n_sp, n_tp),
        out_shape=[pltpu.VMEM((rows, wide), BF16)] * 2,
        in_specs=[hbm, vmem, hbm, hbm, hbm, hbm, hbm, vmem, vmem, vmem, vmem, hbm, hbm],
        out_specs=[vmem, vmem],
        scratch_shapes=[
            pltpu.VMEM((length, model), BF16),
            pltpu.VMEM((5, model, width), BF16),
            pltpu.VMEM((length, width), BF16),
            pltpu.VMEM((length, width), BF16),
            pltpu.VMEM((length + RIM, pool_width), BF16),
            pltpu.VMEM((length, width), BF16),
            pltpu.VMEM((length, width), BF16),
            pltpu.VMEM((pool_width + width, wide), BF16),
            pltpu.VMEM((length, width), BF16),
            pltpu.VMEM((length, width), BF16),
            pltpu.VMEM((length, width), F32),
            pltpu.VMEM((length, pool_width), BF16),
            pltpu.VMEM((CHUNK, width), BF16),
            pltpu.VMEM((CHUNK, width), BF16),
            pltpu.VMEM((length, HEAD_DIM), F32),
            pltpu.VMEM((length, HEAD_DIM), F32),
            pltpu.VMEM((heads, CHUNK, CHUNK), F32),
            pltpu.VMEM((heads, CHUNK, HEAD_DIM), F32),
            pltpu.VMEM((heads, CHUNK, HEAD_DIM), F32),
            pltpu.VMEM((chunks, heads, HEAD_DIM, HEAD_DIM), F32),
            pltpu.VMEM((heads, HEAD_DIM, HEAD_DIM), F32),
            pltpu.VMEM((heads, HEAD_DIM, HEAD_DIM), BF16),
            pltpu.VMEM((heads, HEAD_DIM, HEAD_DIM), BF16),
            pltpu.VMEM((groups, SUB, SUB + RIM), BF16),
            pltpu.VMEM((heads, 8, HEAD_DIM), F32),
            pltpu.VMEM((rows, wide), BF16),
            dma,
            dma((5,)),
            dma((2,)),
            dma((PARTS,)),
            dma((PARTS,)),
            dma((heads,)),
            dma((heads,)),
            dma((2,)),
            dma((per_half,)),
            dma((per_half,)),
        ],
        compiler_params=pltpu.CompilerParams(
            collective_id=0, has_side_effects=True, vmem_limit_bytes=50 * 1024 * 1024
        ),
        cost_estimate=pl.CostEstimate(
            flops=flops, bytes_accessed=20 * 1024 * 1024, transcendentals=0
        ),
    )(
        tokens,
        norm_gain.reshape(1, -1),
        w_pool,
        w_query,
        w_key,
        w_value,
        w_gate,
        pool_mix,
        pool_bias,
        pool_gain.reshape(1, -1),
        ret_gain.reshape(1, -1),
        w_out_pool,
        w_out_ret,
    )
    return (own.astype(F32) + received.astype(F32)).astype(BF16)


def solution(mesh):
    return jax.shard_map(
        per_device,
        mesh=mesh,
        in_specs=(
            P(("fs", "sp", "tp"), None),
            P(),
            P(None, "tp"),
            P(None, "tp"),
            P(None, "tp"),
            P(None, "tp"),
            P(None, "tp"),
            P("tp", None, None),
            P("tp", None),
            P("tp"),
            P("tp"),
            P("tp", None),
            P("tp", None),
        ),
        out_specs=P(("fs", "sp", "tp"), None),
        check_vma=False,
    )
```

profile of v0, /device:TPU:31, one launch (start us, length us, event | category | flops | bytes accessed | tf_op | source)
XLA Modules:
  0.0 37.7 jit_solution(17421623466776403573)
XLA Ops:
  0.0 35.4 %shard_map.127 = (bf16[512,2048]{1,0:T(8,128)(2,1)S(1)}, bf16[512,2048]{1,0:T(8,128)(2,1)S(1)}) custom-call(bf16[512,2048]{1,0:T(8,128)(2,1)} %tokens.1, f32[1,2048]{1,0:T(1,128)} %bitcast.3, bf16[2048,512]{1,0:T(8,128)(2,1)} %w_pool.1, bf16[2048,512]{1,0:T(8,128)(2,1)} %w_query.1, bf16[2048,512]{1,0:T(8,128)(2,1)} %w_key.1, bf16[2048,512]{1,0:T(8,128)(2,1)} %w_value.1, ...), custom_call_target="tpu_custom_call" | custom-call | flops 15032385536 | bytes 20971520 | tf_op jit(solution)/shard_map/pallas_call | solution.py:462
  35.4 2.2 %add_convert_fusion = bf16[512,2048]{1,0:T(8,128)(2,1)} fusion(bf16[512,2048]{1,0:T(8,128)(2,1)S(1)} %get-tuple-element.8, bf16[512,2048]{1,0:T(8,128)(2,1)S(1)} %get-tuple-element.7), kind=kLoop, calls=%fused_computation | loop fusion | flops 4194304 | bytes 6291456 | tf_op jit(solution)/shard_map/convert_element_type | solution.py:526
where the time goes:
time: 37.8 us; the launch traced here: 37.7 us
  Pallas kernels  35.4 us (94%)
  other arithmetic  2.24 us (6%)
    pallas_call x1, Pallas kernels, per_device(): pl.pallas_call(functools.partial(layer_kernel, n_sp, n_tp), out_shape=[pl...  35.4 us
    convert_element_type x1, other arithmetic, per_device(): return (own.astype(F32) + received.astype(F32)).astype(BF16)  2.24 us

commit v1 on v0

v1 whole, which is shorter than its diff:
```python
import functools
import math

import jax
import jax.numpy as jnp
from jax import lax
from jax.experimental import pallas as pl
from jax.experimental.pallas import tpu as pltpu
from jax.sharding import PartitionSpec as P

GROUP_DIM = 256
HEAD_DIM = 128
CHUNK = 256
SUB = 128
RIM = 16
HOP = 4
PIECE = 128
STEP = 16
F32 = jnp.float32
BF16 = jnp.bfloat16
MESH = pl.DeviceIdType.MESH


def dot(a, b):
    return jnp.dot(a, b, preferred_element_type=F32)


def layer_kernel(
    n_sp,
    n_tp,
    tokens,
    norm_gain,
    w_pool,
    w_query,
    w_key,
    w_value,
    w_gate,
    pool_mix,
    pool_bias,
    pool_gain,
    ret_gain,
    w_out_pool,
    w_out_ret,
    out_own,
    x_in,
    tok_own,
    tok_oth,
    wts,
    wo,
    ngain,
    pmix,
    pbias,
    pgain,
    rgain,
    pv,
    pp,
    gated,
    kr,
    qr,
    raw,
    pool_out,
    ret,
    cosine,
    sine,
    decay,
    qdec,
    kdec,
    fresh,
    states,
    total,
    sin_buf,
    sout_buf,
    band,
    ldec,
    acc,
    part_send,
    part_recv,
    x_sem,
    w_sem,
    wo_sem,
    small_sem,
    tok_ss,
    tok_rs,
    st_send,
    st_recv,
    rim_rs,
    part_ss,
    part_rs,
):
    tp = lax.axis_index("tp")
    sp = lax.axis_index("sp")
    rows = tokens.shape[0]
    length = rows * n_tp
    width = w_query.shape[1]
    pool_width = w_pool.shape[1]
    wide = wo.shape[1]
    heads = width // HEAD_DIM
    groups = pool_width // GROUP_DIM
    chunks = length // CHUNK
    per_half = rows // CHUNK
    pieces = rows // PIECE
    seq_len = length * n_sp
    own = pl.multiple_of(tp * rows, rows)
    other = pl.multiple_of((n_tp - 1 - tp) * rows, rows)
    peer = {"tp": n_tp - 1 - tp}

    gain_in = pltpu.make_async_copy(norm_gain, ngain, small_sem.at[0])
    gain_in.start()
    x_copies = []
    for i in range(pieces):
        at = pl.ds(i * PIECE, PIECE)
        x_copies.append(pltpu.make_async_copy(tokens.at[at], x_in.at[at], x_sem.at[i]))
        x_copies[i].start()
    w_in = [
        pltpu.make_async_copy(w, wts.at[i], w_sem.at[i])
        for i, w in enumerate((w_key, w_value, w_pool, w_query, w_gate))
    ]
    smalls = [
        pltpu.make_async_copy(src, dst, small_sem.at[i + 1])
        for i, (src, dst) in enumerate(
            ((pool_mix, pmix), (pool_bias, pbias), (pool_gain, pgain), (ret_gain, rgain))
        )
    ]
    wo_in = [
        pltpu.make_async_copy(w_out_pool, wo.at[pl.ds(0, pool_width)], wo_sem.at[0]),
        pltpu.make_async_copy(w_out_ret, wo.at[pl.ds(pool_width, width)], wo_sem.at[1]),
    ]
    for copy in w_in + smalls + wo_in:
        copy.start()

    barrier = pltpu.get_barrier_semaphore()
    pl.semaphore_signal(barrier, inc=1, device_id=peer, device_id_type=MESH)

    @pl.when(sp > 0)
    def _():
        pl.semaphore_signal(barrier, inc=1, device_id={"sp": sp - 1}, device_id_type=MESH)

    @pl.when(sp < n_sp - 1)
    def _():
        pl.semaphore_signal(barrier, inc=1, device_id={"sp": sp + 1}, device_id_type=MESH)

    def log_decay(h):
        total_heads = heads * n_tp
        value = jnp.float32(0.0)
        for t in range(n_tp):
            one = -(2.0**-5) * (seq_len / 16.0) ** (-2.0 * (t * heads + h) / (total_heads - 1))
            value = jnp.where(tp == t, jnp.float32(one), value)
        return value

    logs = [log_decay(h) for h in range(heads)]
    lane = lax.broadcasted_iota(jnp.int32, (SUB, HEAD_DIM), 1)
    row = lax.broadcasted_iota(jnp.int32, (SUB, HEAD_DIM), 0)
    hd = HEAD_DIM // 2
    low = lane < hd
    freq = jnp.exp(
        jnp.where(low, lane, lane - hd).astype(F32) * (-math.log(10000.0) / hd)
    )
    ang = row.astype(F32) * freq
    cos_r, sin_r = jnp.cos(ang), jnp.sin(ang)
    subs = length // SUB
    base_row = lax.broadcasted_iota(jnp.int32, (subs, HEAD_DIM), 0)
    base = (sp * length + base_row * SUB).astype(F32) * freq[:subs]
    cos_b, sin_b = jnp.cos(base), jnp.sin(base)
    for b in range(subs):
        cb, sb = cos_b[b : b + 1], sin_b[b : b + 1]
        cosine[b * SUB : (b + 1) * SUB] = cb * cos_r - sb * sin_r
        s = sb * cos_r + cb * sin_r
        sine[b * SUB : (b + 1) * SUB] = jnp.where(low, -s, s)

    step_i = lax.broadcasted_iota(jnp.int32, (CHUNK, HEAD_DIM), 0).astype(F32)
    di = lax.broadcasted_iota(jnp.int32, (CHUNK, CHUNK), 0) - lax.broadcasted_iota(
        jnp.int32, (CHUNK, CHUNK), 1
    )
    dpos = jnp.maximum(di, 0).astype(F32)
    for h in range(heads):
        decay[h] = jnp.where(di >= 0, jnp.exp(logs[h] * dpos), 0.0)
        qdec[h] = jnp.exp(logs[h] * (step_i + 1.0))
        kdec[h] = jnp.exp(logs[h] * (CHUNK - 1.0 - step_i))
        ldec[h] = jnp.exp(jnp.full((8, HEAD_DIM), logs[h] * length, F32))
    bi = lax.broadcasted_iota(jnp.int32, (SUB, SUB + RIM), 0)
    bj = lax.broadcasted_iota(jnp.int32, (SUB, SUB + RIM), 1)
    back = bi + RIM - bj
    windows = [jnp.left_shift(jnp.int32(2), tp * groups + g) for g in range(groups)]
    for g in range(groups):
        band[g] = jnp.where((back >= 0) & (back < windows[g]), 1.0, 0.0).astype(BF16)

    sin_buf[heads] = jnp.zeros((HEAD_DIM, HEAD_DIM), BF16)

    @pl.when(sp == 0)
    def _():
        pp[0:RIM] = jnp.zeros((RIM, pool_width), BF16)
        sin_buf[...] = jnp.zeros_like(sin_buf)

    def tok_copy(i):
        at = pl.ds(i * PIECE, PIECE)
        return pltpu.make_async_remote_copy(
            src_ref=tok_own.at[at],
            dst_ref=tok_oth.at[at],
            send_sem=tok_ss.at[i],
            recv_sem=tok_rs.at[i],
            device_id=peer,
            device_id_type=MESH,
        )

    def norm_piece(i):
        starts = range(i * PIECE, (i + 1) * PIECE, STEP)
        scales = []
        for r in starts:
            x = x_in[r : r + STEP, :].astype(F32)
            scales.append(lax.rsqrt(jnp.mean(x * x, axis=-1, keepdims=True) + 1e-06))
        for r, scale in zip(starts, scales):
            x = x_in[r : r + STEP, :].astype(F32)
            tok_own[r : r + STEP, :] = (x * scale * ngain[...]).astype(BF16)

    def rotate(x, at):
        return x * cosine[at] + pltpu.roll(x, HEAD_DIM // 2, 1) * sine[at]

    def place(base_pos, j):
        return pl.multiple_of(base_pos + j * CHUNK, CHUNK)

    def project(w, src, j):
        return dot(src[j * CHUNK : (j + 1) * CHUNK, :], wts[w])

    def kv_chunk(src, base_pos, j):
        start = place(base_pos, j)
        at = pl.ds(start, CHUNK)
        key = project(0, src, j)
        kds = []
        for h in range(heads):
            cols = slice(h * HEAD_DIM, (h + 1) * HEAD_DIM)
            k = rotate(key[:, cols].astype(BF16).astype(F32), at) * HEAD_DIM**-0.5
            kr[at, cols] = k.astype(BF16)
            kds.append((k * kdec[h]).astype(BF16))
        value = project(1, src, j).astype(BF16)
        pv[at] = value
        c = start // CHUNK
        for h in range(heads):
            cols = slice(h * HEAD_DIM, (h + 1) * HEAD_DIM)
            fresh[c, h] = lax.dot_general(
                kds[h], value[:, cols], (((0,), (0,)), ((), ())), preferred_element_type=F32
            )

    def pool_chunk(src, base_pos, j):
        at = pl.ds(pl.multiple_of(place(base_pos, j) + RIM, RIM), CHUNK)
        pp[at] = project(2, src, j).astype(BF16)

    def query_chunk(src, base_pos, j):
        at = pl.ds(place(base_pos, j), CHUNK)
        q = project(3, src, j)
        for h in range(heads):
            cols = slice(h * HEAD_DIM, (h + 1) * HEAD_DIM)
            qr[at, cols] = rotate(q[:, cols].astype(BF16).astype(F32), at).astype(BF16)

    def gate_chunk(src, base_pos, j):
        at = pl.ds(place(base_pos, j), CHUNK)
        g = project(4, src, j).astype(BF16).astype(F32)
        gated[at] = g * (1.0 / (1.0 + jnp.exp(-g))) * rgain[...]

    def intra(base_pos, j):
        at = pl.ds(place(base_pos, j), CHUNK)
        for h in range(heads):
            cols = slice(h * HEAD_DIM, (h + 1) * HEAD_DIM)
            scores = lax.dot_general(
                qr[at, cols], kr[at, cols], (((1,), (1,)), ((), ())), preferred_element_type=F32
            )
            raw[at, cols] = dot((scores * decay[h]).astype(BF16), pv[at, cols])

    def pool_mixing(c):
        for s in range(CHUNK // SUB):
            first = c * CHUNK + s * SUB
            here = sp * length + first + lax.broadcasted_iota(jnp.int32, (SUB, GROUP_DIM), 0)
            for g in range(groups):
                cols = slice(g * GROUP_DIM, (g + 1) * GROUP_DIM)
                span = pp[first : first + SUB + RIM, cols]
                x = pp[first + RIM : first + RIM + SUB, cols].astype(F32)
                count = jnp.minimum(here + 1, windows[g]).astype(F32)
                diff = (dot(band[g], span) / count - x).astype(BF16)
                mixed = dot(diff, pmix[g]) + pbias[g : g + 1]
                pool_out[first : first + SUB, cols] = (mixed * pgain[:, cols]).astype(BF16)

    def st_copy(h):
        return pltpu.make_async_remote_copy(
            src_ref=sout_buf.at[h],
            dst_ref=sin_buf.at[h],
            send_sem=st_send.at[h],
            recv_sem=st_recv.at[h],
            device_id={"sp": sp + 1},
            device_id_type=MESH,
        )

    rim_copy = pltpu.make_async_remote_copy(
        src_ref=pp.at[pl.ds(length, RIM)],
        dst_ref=pp.at[pl.ds(0, RIM)],
        send_sem=rim_rs.at[0],
        recv_sem=rim_rs.at[1],
        device_id={"sp": sp + 1},
        device_id_type=MESH,
    )

    def pass_on(slot, h):
        sout_buf[slot] = (total[h] + ldec[h, 0:1] * sin_buf[slot].astype(F32)).astype(BF16)

    def relay(c):
        h = c - HOP * (sp - 1)
        active = (h >= 0) & (h < heads) & (sp > 0) & (sp < n_sp - 1)
        slot = jnp.where(active, h, heads)

        @pl.when(active)
        def _():
            st_copy(h).wait_recv()

        pass_on(slot, jnp.where(active, h, 0))

        @pl.when(active)
        def _():
            st_copy(h).start()

    slots = 8

    x_copies[0].wait()
    x_copies[1].wait()
    gain_in.wait()
    norm_piece(0)
    neighbours = jnp.where(sp > 0, 1, 0) + jnp.where(sp < n_sp - 1, 1, 0)
    pl.semaphore_wait(barrier, 1 + neighbours)
    tok_copy(0).start()
    norm_piece(1)
    tok_copy(1).start()
    for i in range(2, pieces):
        x_copies[i].wait()
    w_in[0].wait()
    w_in[1].wait()
    kv_chunk(tok_own, own, 0)
    for i in range(2, pieces):
        norm_piece(i)
    for i in range(2, pieces):
        tok_copy(i).start()
    w_in[2].wait()
    for j in range(1, per_half):
        kv_chunk(tok_own, own, j)
    pool_chunk(tok_own, own, 0)
    for i in range(pieces):
        tok_copy(i).wait_recv()
    for j in range(per_half):
        kv_chunk(tok_oth, other, j)

    for h in range(heads):
        step = jnp.exp(jnp.full((1, HEAD_DIM), logs[h] * CHUNK, F32))
        run = fresh[0, h]
        states[0, h] = jnp.zeros((HEAD_DIM, HEAD_DIM), F32)
        for c in range(1, chunks):
            states[c, h] = run
            run = run * step + fresh[c, h]
        total[h] = run
        sout_buf[h] = run.astype(BF16)

    @pl.when((sp == 0) & (sp < n_sp - 1))
    def _():
        for h in range(heads):
            st_copy(h).start()

    w_in[3].wait()
    for j in range(1, per_half):
        pool_chunk(tok_own, own, j)
    for j in range(per_half):
        pool_chunk(tok_oth, other, j)

    @pl.when(sp < n_sp - 1)
    def _():
        rim_copy.start()

    for copy in w_in[4:] + smalls:
        copy.wait()

    query_chunk(tok_own, own, 0)
    query_chunk(tok_own, own, 1)
    relay(0)
    query_chunk(tok_oth, other, 0)
    relay(1)
    query_chunk(tok_oth, other, 1)
    relay(2)
    gate_chunk(tok_own, own, 0)
    intra(own, 0)
    pool_mixing(1)
    relay(3)
    gate_chunk(tok_own, own, 1)
    intra(own, 1)
    pool_mixing(2)
    relay(4)
    gate_chunk(tok_oth, other, 0)
    intra(other, 0)
    pool_mixing(3)
    relay(5)

    @pl.when(sp > 0)
    def _():
        rim_copy.wait_recv()

    gate_chunk(tok_oth, other, 1)
    intra(other, 1)
    pool_mixing(0)
    for copy in wo_in:
        copy.wait()
    relay(6)

    tile = 512

    def pool_share(base_pos, j):
        at = pl.ds(place(base_pos, j), CHUNK)
        mine = slice(j * CHUNK, (j + 1) * CHUNK)
        for n in range(wide // tile):
            cols = slice(n * tile, (n + 1) * tile)
            acc[mine, cols] = dot(pool_out[at, :], wo[:pool_width, cols])

    pool_share(other, 0)
    relay(7)
    pool_share(other, 1)

    def rest(h, carry):
        late = (h + HOP * (sp - 1) >= slots) | (sp == n_sp - 1)

        @pl.when(late & (sp > 0))
        def _():
            st_copy(h).wait_recv()

            @pl.when(sp < n_sp - 1)
            def _():
                pass_on(h, h)
                st_copy(h).start()

        return carry

    lax.fori_loop(0, heads, rest, 0)

    def finish(base_pos, j):
        start = place(base_pos, j)
        at = pl.ds(start, CHUNK)
        c = start // CHUNK
        for h in range(heads):
            cols = slice(h * HEAD_DIM, (h + 1) * HEAD_DIM)
            ahead = jnp.exp(jnp.full((1, HEAD_DIM), logs[h], F32) * start.astype(F32))
            state = (states[c, h] + sin_buf[h].astype(F32) * ahead).astype(BF16)
            r = raw[at, cols] + qdec[h] * dot(qr[at, cols], state)
            r = r - jnp.mean(r, axis=-1, keepdims=True)
            var = jnp.mean(r * r, axis=-1, keepdims=True)
            ret[at, cols] = (gated[at, cols] * (r * lax.rsqrt(var + 1e-06))).astype(BF16)

    def part_copy(j):
        at = pl.ds(j * CHUNK, CHUNK)
        return pltpu.make_async_remote_copy(
            src_ref=part_send.at[at],
            dst_ref=part_recv.at[at],
            send_sem=part_ss.at[j],
            recv_sem=part_rs.at[j],
            device_id=peer,
            device_id_type=MESH,
        )

    def multiply_other(j):
        at = pl.ds(place(other, j), CHUNK)
        mine = slice(j * CHUNK, (j + 1) * CHUNK)
        for n in range(wide // tile):
            cols = slice(n * tile, (n + 1) * tile)
            part_send[mine, cols] = (
                acc[mine, cols] + dot(ret[at, :], wo[pool_width:, cols])
            ).astype(BF16)

    def multiply_own(j):
        at = pl.ds(place(own, j), CHUNK)
        mine = slice(j * CHUNK, (j + 1) * CHUNK)
        left = jnp.concatenate([pool_out[at, :], ret[at, :]], axis=1)
        for n in range(wide // tile):
            cols = slice(n * tile, (n + 1) * tile)
            out_own[mine, cols] = dot(left, wo[:, cols]).astype(BF16)

    def add_received(j):
        mine = slice(j * CHUNK, (j + 1) * CHUNK)
        out_own[mine] = (out_own[mine].astype(F32) + part_recv[mine].astype(F32)).astype(BF16)

    finish(other, 0)
    for j in range(per_half):
        multiply_other(j)
        if j + 1 < per_half:
            finish(other, j + 1)
        else:
            finish(own, 0)
        part_copy(j).start()
    for j in range(per_half):
        multiply_own(j)
        if j > 0:
            add_received(j - 1)
        if j + 1 < per_half:
            finish(own, j + 1)
        part_copy(j).wait_recv()
    add_received(per_half - 1)

    for i in range(pieces):
        tok_copy(i).wait_send()
    for j in range(per_half):
        part_copy(j).wait_send()

    @pl.when(sp < n_sp - 1)
    def _():
        rim_copy.wait_send()
        for h in range(heads):
            st_copy(h).wait_send()


def per_device(
    tokens,
    norm_gain,
    w_pool,
    w_query,
    w_key,
    w_value,
    w_gate,
    pool_mix,
    pool_bias,
    pool_gain,
    ret_gain,
    w_out_pool,
    w_out_ret,
):
    n_sp, n_tp = lax.axis_size("sp"), lax.axis_size("tp")
    rows, model = tokens.shape
    length = rows * n_tp
    width = w_query.shape[1]
    heads = width // HEAD_DIM
    pool_width = w_pool.shape[1]
    groups = pool_width // GROUP_DIM
    chunks = length // CHUNK
    per_half = rows // CHUNK
    pieces = rows // PIECE
    wide = w_out_pool.shape[1]
    hbm = pl.BlockSpec(memory_space=pltpu.HBM)
    vmem = pl.BlockSpec(memory_space=pltpu.VMEM)
    dma = pltpu.SemaphoreType.DMA
    flops = 2 * length * model * (pool_width + 4 * width) + 2 * length * (pool_width + width) * wide
    return pl.pallas_call(
        functools.partial(layer_kernel, n_sp, n_tp),
        out_shape=pltpu.VMEM((rows, wide), BF16),
        in_specs=[hbm] * 13,
        out_specs=vmem,
        scratch_shapes=[
            pltpu.VMEM((rows, model), BF16),
            pltpu.VMEM((rows, model), BF16),
            pltpu.VMEM((rows, model), BF16),
            pltpu.VMEM((5, model, width), BF16),
            pltpu.VMEM((pool_width + width, wide), BF16),
            pltpu.VMEM((1, model), F32),
            pltpu.VMEM((groups, GROUP_DIM, GROUP_DIM), BF16),
            pltpu.VMEM((groups, GROUP_DIM), F32),
            pltpu.VMEM((1, pool_width), F32),
            pltpu.VMEM((1, width), F32),
            pltpu.VMEM((length, width), BF16),
            pltpu.VMEM((length + RIM, pool_width), BF16),
            pltpu.VMEM((length, width), F32),
            pltpu.VMEM((length, width), BF16),
            pltpu.VMEM((length, width), BF16),
            pltpu.VMEM((length, width), F32),
            pltpu.VMEM((length, pool_width), BF16),
            pltpu.VMEM((length, width), BF16),
            pltpu.VMEM((length, HEAD_DIM), F32),
            pltpu.VMEM((length, HEAD_DIM), F32),
            pltpu.VMEM((heads, CHUNK, CHUNK), F32),
            pltpu.VMEM((heads, CHUNK, HEAD_DIM), F32),
            pltpu.VMEM((heads, CHUNK, HEAD_DIM), F32),
            pltpu.VMEM((chunks, heads, HEAD_DIM, HEAD_DIM), F32),
            pltpu.VMEM((chunks, heads, HEAD_DIM, HEAD_DIM), F32),
            pltpu.VMEM((heads, HEAD_DIM, HEAD_DIM), F32),
            pltpu.VMEM((heads + 1, HEAD_DIM, HEAD_DIM), BF16),
            pltpu.VMEM((heads + 1, HEAD_DIM, HEAD_DIM), BF16),
            pltpu.VMEM((groups, SUB, SUB + RIM), BF16),
            pltpu.VMEM((heads, 8, HEAD_DIM), F32),
            pltpu.VMEM((rows, wide), F32),
            pltpu.VMEM((rows, wide), BF16),
            pltpu.VMEM((rows, wide), BF16),
            dma((pieces,)),
            dma((5,)),
            dma((2,)),
            dma((5,)),
            dma((pieces,)),
            dma((pieces,)),
            dma((heads,)),
            dma((heads,)),
            dma((2,)),
            dma((per_half,)),
            dma((per_half,)),
        ],
        compiler_params=pltpu.CompilerParams(
            collective_id=0, has_side_effects=True, vmem_limit_bytes=56 * 1024 * 1024
        ),
        cost_estimate=pl.CostEstimate(
            flops=flops, bytes_accessed=20 * 1024 * 1024, transcendentals=0
        ),
    )(
        tokens,
        norm_gain.reshape(1, -1),
        w_pool,
        w_query,
        w_key,
        w_value,
        w_gate,
        pool_mix,
        pool_bias,
        pool_gain.reshape(1, -1),
        ret_gain.reshape(1, -1),
        w_out_pool,
        w_out_ret,
    )


def solution(mesh):
    return jax.shard_map(
        per_device,
        mesh=mesh,
        in_specs=(
            P(("fs", "sp", "tp"), None),
            P(),
            P(None, "tp"),
            P(None, "tp"),
            P(None, "tp"),
            P(None, "tp"),
            P(None, "tp"),
            P("tp", None, None),
            P("tp", None),
            P("tp"),
            P("tp"),
            P("tp", None),
            P("tp", None),
        ),
        out_specs=P(("fs", "sp", "tp"), None),
        check_vma=False,
    )
```

time: 37.8 us -> 33.6 us (0.89)
  Pallas kernels: 35.4 us -> 32.2 us
  other arithmetic: 2.24 us -> 0 us
  local copies, waits for them, and re-layouts: 0 us -> 1.32 us
    pallas_call x1, Pallas kernels: 35.4 us -> 32.2 us  [per_device(): pl.pallas_call(functools.partial(layer_kernel, n_sp, n_tp), out_shape=plt...]
    convert_element_type x1 -> x0, other arithmetic: 2.24 us -> none  [per_device(): return (own.astype(F32) + received.astype(F32)).astype(BF16)]
    unnamed x0 -> x1, local copies, waits for them, and re-layouts: none -> 1.32 us
where the time goes in v1:
time: 33.6 us; the launch traced here: 33.5 us
  Pallas kernels  32.2 us (96%)
  local copies, waits for them, and re-layouts  1.32 us (4%)
    pallas_call x1, Pallas kernels, per_device(): pl.pallas_call(functools.partial(layer_kernel, n_sp, n_tp), out_shape=plt...  32.2 us
    unnamed x1, local copies, waits for them, and re-layouts  1.32 us

profile of v1, /device:TPU:31, one launch (start us, length us, event | category | flops | bytes accessed | tf_op | source)
XLA Modules:
  0.0 33.5 jit_solution(4204568973447780932)
XLA Ops:
  0.0 32.2 %shard_map.127 = bf16[512,2048]{1,0:T(8,128)(2,1)S(1)} custom-call(bf16[512,2048]{1,0:T(8,128)(2,1)} %tokens.1, f32[1,2048]{1,0:T(1,128)} %bitcast.3, bf16[2048,512]{1,0:T(8,128)(2,1)} %w_pool.1, bf16[2048,512]{1,0:T(8,128)(2,1)} %w_query.1, bf16[2048,512]{1,0:T(8,128)(2,1)} %w_key.1, bf16[2048,512]{1,0:T(8,128)(2,1)} %w_value.1, bf16[2048,512]{1,0:T(8,128)(2,1)} %w_gate.1, ...), custom_call_target="tpu_custom_call" | custom-call | flops 15032385536 | bytes 20971520 | tf_op jit(solution)/shard_map/pallas_call | solution.py:539
  32.2 1.3 %copy.15 = bf16[512,2048]{1,0:T(8,128)(2,1)} copy(bf16[512,2048]{1,0:T(8,128)(2,1)S(1)} %shard_map.127) | data formatting | bytes 4194304

commit v2 on v1

--- a/solution.py
+++ b/solution.py
@@ -16,6 +16,7 @@
 HOP = 4
 PIECE = 128
 STEP = 16
+TILE = 512
 F32 = jnp.float32
 BF16 = jnp.bfloat16
 MESH = pl.DeviceIdType.MESH
@@ -56,8 +57,11 @@
     pp,
     gated,
     kr,
+    kd,
     qr,
+    weights,
     raw,
+    pool_diff,
     pool_out,
     ret,
     cosine,
@@ -93,7 +97,9 @@
     length = rows * n_tp
     width = w_query.shape[1]
     pool_width = w_pool.shape[1]
-    wide = wo.shape[1]
+    wide = w_out_pool.shape[1]
+    tiles = wide // TILE
+    blocks = tokens.shape[1] // TILE
     heads = width // HEAD_DIM
     groups = pool_width // GROUP_DIM
     chunks = length // CHUNK
@@ -122,11 +128,17 @@
         )
     ]
     wo_in = [
-        pltpu.make_async_copy(w_out_pool, wo.at[pl.ds(0, pool_width)], wo_sem.at[0]),
-        pltpu.make_async_copy(w_out_ret, wo.at[pl.ds(pool_width, width)], wo_sem.at[1]),
+        pltpu.make_async_copy(
+            src.at[:, pl.ds(n * TILE, TILE)],
+            wo.at[n, pl.ds(low, src.shape[0])],
+            wo_sem.at[i, n],
+        )
+        for i, (src, low) in enumerate(((w_out_pool, 0), (w_out_ret, pool_width)))
+        for n in range(tiles)
     ]
-    for copy in w_in + smalls + wo_in:
-        copy.start()
+    w_in[0].start()
+    for copy in w_in[1:]:
+        copy.start(priority=1)
 
     barrier = pltpu.get_barrier_semaphore()
     pl.semaphore_signal(barrier, inc=1, device_id=peer, device_id_type=MESH)
@@ -194,8 +206,8 @@
     def tok_copy(i):
         at = pl.ds(i * PIECE, PIECE)
         return pltpu.make_async_remote_copy(
-            src_ref=tok_own.at[at],
-            dst_ref=tok_oth.at[at],
+            src_ref=tok_own.at[:, at],
+            dst_ref=tok_oth.at[:, at],
             send_sem=tok_ss.at[i],
             recv_sem=tok_rs.at[i],
             device_id=peer,
@@ -210,73 +222,109 @@
             scales.append(lax.rsqrt(jnp.mean(x * x, axis=-1, keepdims=True) + 1e-06))
         for r, scale in zip(starts, scales):
             x = x_in[r : r + STEP, :].astype(F32)
-            tok_own[r : r + STEP, :] = (x * scale * ngain[...]).astype(BF16)
+            normed = (x * scale * ngain[...]).astype(BF16)
+            for n in range(blocks):
+                tok_own[n, r : r + STEP, :] = normed[:, n * TILE : (n + 1) * TILE]
 
     def rotate(x, at):
         return x * cosine[at] + pltpu.roll(x, HEAD_DIM // 2, 1) * sine[at]
 
-    def place(base_pos, j):
-        return pl.multiple_of(base_pos + j * CHUNK, CHUNK)
-
-    def project(w, src, j):
-        return dot(src[j * CHUNK : (j + 1) * CHUNK, :], wts[w])
-
-    def kv_chunk(src, base_pos, j):
-        start = place(base_pos, j)
+    half = blocks // 2
+    own_at = [(tok_own, own, j) for j in range(per_half)]
+    oth_at = [(tok_oth, other, j) for j in range(per_half)]
+
+    def position(unit):
+        return pl.multiple_of(unit[1] + unit[2] * CHUNK, CHUNK)
+
+    def project(w, unit, lo=0, hi=blocks, res=None):
+        src, _, j = unit
+        mine = slice(j * CHUNK, (j + 1) * CHUNK)
+        for n in range(lo, hi):
+            term = dot(src[n, mine, :], wts[w, n * TILE : (n + 1) * TILE, :])
+            res = term if res is None else res + term
+        return res
+
+    def split(w, unit, between):
+        res = project(w, unit, 0, half)
+        between()
+        return project(w, unit, half, blocks, res)
+
+    def nothing():
+        pass
+
+    def head_cols(h):
+        return slice(h * HEAD_DIM, (h + 1) * HEAD_DIM)
+
+    def key_unit(unit, between=nothing):
+        at = pl.ds(position(unit), CHUNK)
+        key = split(0, unit, between)
+        for h in range(heads):
+            k = rotate(key[:, head_cols(h)].astype(BF16).astype(F32), at) * HEAD_DIM**-0.5
+            kr[at, head_cols(h)] = k.astype(BF16)
+            kd[at, head_cols(h)] = (k * kdec[h]).astype(BF16)
+
+    def value_unit(unit, between=nothing):
+        pv[pl.ds(position(unit), CHUNK)] = split(1, unit, between).astype(BF16)
+
+    def state_unit(unit):
+        start = position(unit)
         at = pl.ds(start, CHUNK)
-        key = project(0, src, j)
-        kds = []
-        for h in range(heads):
-            cols = slice(h * HEAD_DIM, (h + 1) * HEAD_DIM)
-            k = rotate(key[:, cols].astype(BF16).astype(F32), at) * HEAD_DIM**-0.5
-            kr[at, cols] = k.astype(BF16)
-            kds.append((k * kdec[h]).astype(BF16))
-        value = project(1, src, j).astype(BF16)
-        pv[at] = value
-        c = start // CHUNK
-        for h in range(heads):
-            cols = slice(h * HEAD_DIM, (h + 1) * HEAD_DIM)
-            fresh[c, h] = lax.dot_general(
-                kds[h], value[:, cols], (((0,), (0,)), ((), ())), preferred_element_type=F32
+        for h in range(heads):
+            fresh[start // CHUNK, h] = lax.dot_general(
+                kd[at, head_cols(h)],
+                pv[at, head_cols(h)],
+                (((0,), (0,)), ((), ())),
+                preferred_element_type=F32,
             )
 
-    def pool_chunk(src, base_pos, j):
-        at = pl.ds(pl.multiple_of(place(base_pos, j) + RIM, RIM), CHUNK)
-        pp[at] = project(2, src, j).astype(BF16)
-
-    def query_chunk(src, base_pos, j):
-        at = pl.ds(place(base_pos, j), CHUNK)
-        q = project(3, src, j)
-        for h in range(heads):
-            cols = slice(h * HEAD_DIM, (h + 1) * HEAD_DIM)
-            qr[at, cols] = rotate(q[:, cols].astype(BF16).astype(F32), at).astype(BF16)
-
-    def gate_chunk(src, base_pos, j):
-        at = pl.ds(place(base_pos, j), CHUNK)
-        g = project(4, src, j).astype(BF16).astype(F32)
+    def pool_unit(unit, between=nothing):
+        at = pl.ds(pl.multiple_of(position(unit) + RIM, RIM), CHUNK)
+        pp[at] = split(2, unit, between).astype(BF16)
+
+    def query_unit(unit, between=nothing):
+        at = pl.ds(position(unit), CHUNK)
+        q = split(3, unit, between)
+        for h in range(heads):
+            qr[at, head_cols(h)] = rotate(q[:, head_cols(h)].astype(BF16).astype(F32), at).astype(BF16)
+
+    def gate_unit(unit, between=nothing):
+        at = pl.ds(position(unit), CHUNK)
+        g = split(4, unit, between).astype(BF16).astype(F32)
         gated[at] = g * (1.0 / (1.0 + jnp.exp(-g))) * rgain[...]
 
-    def intra(base_pos, j):
-        at = pl.ds(place(base_pos, j), CHUNK)
-        for h in range(heads):
-            cols = slice(h * HEAD_DIM, (h + 1) * HEAD_DIM)
+    def score_unit(unit):
+        at = pl.ds(position(unit), CHUNK)
+        for h in range(heads):
             scores = lax.dot_general(
-                qr[at, cols], kr[at, cols], (((1,), (1,)), ((), ())), preferred_element_type=F32
+                qr[at, head_cols(h)],
+                kr[at, head_cols(h)],
+                (((1,), (1,)), ((), ())),
+                preferred_element_type=F32,
             )
-            raw[at, cols] = dot((scores * decay[h]).astype(BF16), pv[at, cols])
+            weights[h] = (scores * decay[h]).astype(BF16)
+
+    def intra_unit(unit):
+        at = pl.ds(position(unit), CHUNK)
+        for h in range(heads):
+            raw[at, head_cols(h)] = dot(weights[h], pv[at, head_cols(h)])
+
+    def pool_pieces(c):
+        for i in range(CHUNK // SUB):
+            for g in range(groups):
+                yield c * CHUNK + i * SUB, g, slice(g * GROUP_DIM, (g + 1) * GROUP_DIM)
+
+    def pool_windows(c):
+        for first, g, cols in pool_pieces(c):
+            here = sp * length + first + lax.broadcasted_iota(jnp.int32, (SUB, GROUP_DIM), 0)
+            span = pp[first : first + SUB + RIM, cols]
+            x = pp[first + RIM : first + RIM + SUB, cols].astype(F32)
+            count = jnp.minimum(here + 1, windows[g]).astype(F32)
+            pool_diff[first : first + SUB, cols] = (dot(band[g], span) / count - x).astype(BF16)
 
     def pool_mixing(c):
-        for s in range(CHUNK // SUB):
-            first = c * CHUNK + s * SUB
-            here = sp * length + first + lax.broadcasted_iota(jnp.int32, (SUB, GROUP_DIM), 0)
-            for g in range(groups):
-                cols = slice(g * GROUP_DIM, (g + 1) * GROUP_DIM)
-                span = pp[first : first + SUB + RIM, cols]
-                x = pp[first + RIM : first + RIM + SUB, cols].astype(F32)
-                count = jnp.minimum(here + 1, windows[g]).astype(F32)
-                diff = (dot(band[g], span) / count - x).astype(BF16)
-                mixed = dot(diff, pmix[g]) + pbias[g : g + 1]
-                pool_out[first : first + SUB, cols] = (mixed * pgain[:, cols]).astype(BF16)
+        for first, g, cols in pool_pieces(c):
+            mixed = dot(pool_diff[first : first + SUB, cols], pmix[g]) + pbias[g : g + 1]
+            pool_out[first : first + SUB, cols] = (mixed * pgain[:, cols]).astype(BF16)
 
     def st_copy(h):
         return pltpu.make_async_remote_copy(
@@ -317,105 +365,115 @@
 
     slots = 8
 
+    gain_in.wait()
     x_copies[0].wait()
-    x_copies[1].wait()
-    gain_in.wait()
     norm_piece(0)
     neighbours = jnp.where(sp > 0, 1, 0) + jnp.where(sp < n_sp - 1, 1, 0)
     pl.semaphore_wait(barrier, 1 + neighbours)
     tok_copy(0).start()
-    norm_piece(1)
-    tok_copy(1).start()
-    for i in range(2, pieces):
+    for i in range(1, pieces):
         x_copies[i].wait()
+        norm_piece(i)
+        tok_copy(i).start()
     w_in[0].wait()
     w_in[1].wait()
-    kv_chunk(tok_own, own, 0)
-    for i in range(2, pieces):
-        norm_piece(i)
-    for i in range(2, pieces):
-        tok_copy(i).start()
-    w_in[2].wait()
-    for j in range(1, per_half):
-        kv_chunk(tok_own, own, j)
-    pool_chunk(tok_own, own, 0)
-    for i in range(pieces):
-        tok_copy(i).wait_recv()
-    for j in range(per_half):
-        kv_chunk(tok_oth, other, j)
-
-    for h in range(heads):
-        step = jnp.exp(jnp.full((1, HEAD_DIM), logs[h] * CHUNK, F32))
-        run = fresh[0, h]
-        states[0, h] = jnp.zeros((HEAD_DIM, HEAD_DIM), F32)
-        for c in range(1, chunks):
-            states[c, h] = run
-            run = run * step + fresh[c, h]
-        total[h] = run
-        sout_buf[h] = run.astype(BF16)
+    for copy in smalls + wo_in:
+        copy.start(priority=1)
+    for copy in w_in[2:4]:
+        copy.wait()
+    per_chunk = CHUNK // PIECE
+
+    def arrive(j):
+        def wait():
+            for i in range(j * per_chunk, (j + 1) * per_chunk):
+                tok_copy(i).wait_recv()
+
+        return wait
+
+    units = own_at + oth_at
+    before = None
+    for i, unit in enumerate(units):
+        key_unit(unit, functools.partial(state_unit, before) if i > 0 else nothing)
+        nxt = i + 1 - per_half
+        value_unit(unit, arrive(nxt) if 0 <= nxt < per_half else nothing)
+        before = unit
+
+    def combine():
+        state_unit(before)
+        for h in range(heads):
+            step = jnp.exp(jnp.full((1, HEAD_DIM), logs[h] * CHUNK, F32))
+            run = fresh[0, h]
+            states[0, h] = jnp.zeros((HEAD_DIM, HEAD_DIM), F32)
+            for c in range(1, chunks):
+                states[c, h] = run
+                run = run * step + fresh[c, h]
+            total[h] = run
+            sout_buf[h] = run.astype(BF16)
+
+    pool_unit(units[0], combine)
 
     @pl.when((sp == 0) & (sp < n_sp - 1))
     def _():
         for h in range(heads):
             st_copy(h).start()
 
-    w_in[3].wait()
-    for j in range(1, per_half):
-        pool_chunk(tok_own, own, j)
-    for j in range(per_half):
-        pool_chunk(tok_oth, other, j)
-
-    @pl.when(sp < n_sp - 1)
-    def _():
-        rim_copy.start()
+    for unit in units[1:]:
+        pool_unit(unit)
+
+    def send_rim():
+        @pl.when(sp < n_sp - 1)
+        def _():
+            rim_copy.start()
 
     for copy in w_in[4:] + smalls:
         copy.wait()
 
-    query_chunk(tok_own, own, 0)
-    query_chunk(tok_own, own, 1)
-    relay(0)
-    query_chunk(tok_oth, other, 0)
-    relay(1)
-    query_chunk(tok_oth, other, 1)
-    relay(2)
-    gate_chunk(tok_own, own, 0)
-    intra(own, 0)
-    pool_mixing(1)
-    relay(3)
-    gate_chunk(tok_own, own, 1)
-    intra(own, 1)
-    pool_mixing(2)
-    relay(4)
-    gate_chunk(tok_oth, other, 0)
-    intra(other, 0)
-    pool_mixing(3)
-    relay(5)
-
-    @pl.when(sp > 0)
-    def _():
-        rim_copy.wait_recv()
-
-    gate_chunk(tok_oth, other, 1)
-    intra(other, 1)
-    pool_mixing(0)
+    query_unit(units[0], send_rim)
+    query_unit(units[1])
+    query_unit(units[2], functools.partial(relay, 0))
+    query_unit(units[3], functools.partial(relay, 1))
+
+    def mid(unit, c, fence):
+        def run():
+            fence()
+            intra_unit(unit)
+            pool_windows(c)
+
+        return run
+
+    def relays(*cs):
+        def run():
+            for c in cs:
+                relay(c)
+
+        return run
+
+    def rim_wait():
+        relay(6)
+        relay(7)
+
+        @pl.when(sp > 0)
+        def _():
+            rim_copy.wait_recv()
+
+    fences = [relays(2), relays(3, 4), relays(5), rim_wait]
+    for i, unit in enumerate(units):
+        c = (i + 1) % chunks
+        score_unit(unit)
+        gate_unit(unit, mid(unit, c, fences[i]))
+        pool_mixing(c)
     for copy in wo_in:
         copy.wait()
-    relay(6)
-
-    tile = 512
-
-    def pool_share(base_pos, j):
-        at = pl.ds(place(base_pos, j), CHUNK)
+
+    def pool_share(j):
+        at = pl.ds(position(oth_at[j]), CHUNK)
         mine = slice(j * CHUNK, (j + 1) * CHUNK)
-        for n in range(wide // tile):
-            cols = slice(n * tile, (n + 1) * tile)
-            acc[mine, cols] = dot(pool_out[at, :], wo[:pool_width, cols])
-
-    pool_share(other, 0)
-    relay(7)
-    pool_share(other, 1)
-
+        for n in range(tiles):
+            cols = slice(n * TILE, (n + 1) * TILE)
+            acc[mine, cols] = dot(pool_out[at, :], wo[n, :pool_width, :])
+
+    for j in range(per_half - 1):
+        pool_share(j)
     def rest(h, carry):
         late = (h + HOP * (sp - 1) >= slots) | (sp == n_sp - 1)
 
@@ -432,12 +490,12 @@
 
     lax.fori_loop(0, heads, rest, 0)
 
-    def finish(base_pos, j):
-        start = place(base_pos, j)
+    def finish(unit):
+        start = position(unit)
         at = pl.ds(start, CHUNK)
         c = start // CHUNK
         for h in range(heads):
-            cols = slice(h * HEAD_DIM, (h + 1) * HEAD_DIM)
+            cols = head_cols(h)
             ahead = jnp.exp(jnp.full((1, HEAD_DIM), logs[h], F32) * start.astype(F32))
             state = (states[c, h] + sin_buf[h].astype(F32) * ahead).astype(BF16)
             r = raw[at, cols] + qdec[h] * dot(qr[at, cols], state)
@@ -456,42 +514,44 @@
             device_id_type=MESH,
         )
 
-    def multiply_other(j):
-        at = pl.ds(place(other, j), CHUNK)
+    def multiply_other(j, n):
+        at = pl.ds(position(oth_at[j]), CHUNK)
         mine = slice(j * CHUNK, (j + 1) * CHUNK)
-        for n in range(wide // tile):
-            cols = slice(n * tile, (n + 1) * tile)
-            part_send[mine, cols] = (
-                acc[mine, cols] + dot(ret[at, :], wo[pool_width:, cols])
-            ).astype(BF16)
-
-    def multiply_own(j):
-        at = pl.ds(place(own, j), CHUNK)
+        cols = slice(n * TILE, (n + 1) * TILE)
+        part_send[mine, cols] = (
+            acc[mine, cols] + dot(ret[at, :], wo[n, pool_width:, :])
+        ).astype(BF16)
+
+    def multiply_own(j, n):
+        at = pl.ds(position(own_at[j]), CHUNK)
         mine = slice(j * CHUNK, (j + 1) * CHUNK)
-        left = jnp.concatenate([pool_out[at, :], ret[at, :]], axis=1)
-        for n in range(wide // tile):
-            cols = slice(n * tile, (n + 1) * tile)
-            out_own[mine, cols] = dot(left, wo[:, cols]).astype(BF16)
+        cols = slice(n * TILE, (n + 1) * TILE)
+        out_own[mine, cols] = (
+            dot(pool_out[at, :], wo[n, :pool_width, :]) + dot(ret[at, :], wo[n, pool_width:, :])
+        ).astype(BF16)
 
     def add_received(j):
         mine = slice(j * CHUNK, (j + 1) * CHUNK)
         out_own[mine] = (out_own[mine].astype(F32) + part_recv[mine].astype(F32)).astype(BF16)
 
-    finish(other, 0)
-    for j in range(per_half):
-        multiply_other(j)
-        if j + 1 < per_half:
-            finish(other, j + 1)
-        else:
-            finish(own, 0)
-        part_copy(j).start()
-    for j in range(per_half):
-        multiply_own(j)
-        if j > 0:
-            add_received(j - 1)
-        if j + 1 < per_half:
-            finish(own, j + 1)
-        part_copy(j).wait_recv()
+    order = oth_at + own_at
+    finish(order[0])
+    pool_share(per_half - 1)
+    for i in range(len(order)):
+        sending = i < per_half
+        for n in range(tiles):
+            if n == 1 and 0 < i <= per_half:
+                part_copy(i - 1).start()
+            if n == 1 and i > per_half:
+                part_copy(i - 1 - per_half).wait_recv()
+                add_received(i - 1 - per_half)
+            if n == 2 and i + 1 < len(order):
+                finish(order[i + 1])
+            if sending:
+                multiply_other(i, n)
+            else:
+                multiply_own(i - per_half, n)
+    part_copy(per_half - 1).wait_recv()
     add_received(per_half - 1)
 
     for i in range(pieces):
@@ -543,10 +603,10 @@
         out_specs=vmem,
         scratch_shapes=[
             pltpu.VMEM((rows, model), BF16),
-            pltpu.VMEM((rows, model), BF16),
-            pltpu.VMEM((rows, model), BF16),
+            pltpu.VMEM((model // TILE, rows, TILE), BF16),
+            pltpu.VMEM((model // TILE, rows, TILE), BF16),
             pltpu.VMEM((5, model, width), BF16),
-            pltpu.VMEM((pool_width + width, wide), BF16),
+            pltpu.VMEM((wide // TILE, pool_width + width, TILE), BF16),
             pltpu.VMEM((1, model), F32),
             pltpu.VMEM((groups, GROUP_DIM, GROUP_DIM), BF16),
             pltpu.VMEM((groups, GROUP_DIM), F32),
@@ -557,7 +617,10 @@
             pltpu.VMEM((length, width), F32),
             pltpu.VMEM((length, width), BF16),
             pltpu.VMEM((length, width), BF16),
+            pltpu.VMEM((length, width), BF16),
+            pltpu.VMEM((heads, CHUNK, CHUNK), BF16),
             pltpu.VMEM((length, width), F32),
+            pltpu.VMEM((length, pool_width), BF16),
             pltpu.VMEM((length, pool_width), BF16),
             pltpu.VMEM((length, width), BF16),
             pltpu.VMEM((length, HEAD_DIM), F32),
@@ -577,7 +640,7 @@
             pltpu.VMEM((rows, wide), BF16),
             dma((pieces,)),
             dma((5,)),
-            dma((2,)),
+            dma((2, wide // TILE)),
             dma((5,)),
             dma((pieces,)),
             dma((pieces,)),

time: 33.6 us -> 28.6 us (0.85)
  Pallas kernels: 32.2 us -> 27.1 us
    pallas_call x1, Pallas kernels: 32.2 us -> 27.1 us  [per_device(): pl.pallas_call(functools.partial(layer_kernel, n_sp, n_tp), out_shape=plt...]
where the time goes in v2:
time: 28.6 us; the launch traced here: 28.4 us
  Pallas kernels  27.1 us (95%)
  local copies, waits for them, and re-layouts  1.32 us (5%)
    pallas_call x1, Pallas kernels, per_device(): pl.pallas_call(functools.partial(layer_kernel, n_sp, n_tp), out_shape=plt...  27.1 us
    unnamed x1, local copies, waits for them, and re-layouts  1.32 us

profile of v2, /device:TPU:31, one launch (start us, length us, event | category | flops | bytes accessed | tf_op | source)
XLA Modules:
  0.0 28.4 jit_solution(6465652282326659999)
XLA Ops:
  0.0 27.1 %shard_map.127 = bf16[512,2048]{1,0:T(8,128)(2,1)S(1)} custom-call(bf16[512,2048]{1,0:T(8,128)(2,1)} %tokens.1, f32[1,2048]{1,0:T(1,128)} %bitcast.3, bf16[2048,512]{1,0:T(8,128)(2,1)} %w_pool.1, bf16[2048,512]{1,0:T(8,128)(2,1)} %w_query.1, bf16[2048,512]{1,0:T(8,128)(2,1)} %w_key.1, bf16[2048,512]{1,0:T(8,128)(2,1)} %w_value.1, bf16[2048,512]{1,0:T(8,128)(2,1)} %w_gate.1, ...), custom_call_target="tpu_custom_call" | custom-call | flops 15032385536 | bytes 20971520 | tf_op jit(solution)/shard_map/pallas_call | solution.py:599
  27.1 1.3 %copy.15 = bf16[512,2048]{1,0:T(8,128)(2,1)} copy(bf16[512,2048]{1,0:T(8,128)(2,1)S(1)} %shard_map.127) | data formatting | bytes 4194304

commit v3 on v2

--- a/solution.py
+++ b/solution.py
@@ -136,8 +136,7 @@
         for i, (src, low) in enumerate(((w_out_pool, 0), (w_out_ret, pool_width)))
         for n in range(tiles)
     ]
-    w_in[0].start()
-    for copy in w_in[1:]:
+    for copy in w_in:
         copy.start(priority=1)
 
     barrier = pltpu.get_barrier_semaphore()
@@ -371,31 +370,44 @@
     neighbours = jnp.where(sp > 0, 1, 0) + jnp.where(sp < n_sp - 1, 1, 0)
     pl.semaphore_wait(barrier, 1 + neighbours)
     tok_copy(0).start()
-    for i in range(1, pieces):
+    per_chunk = CHUNK // PIECE
+    for i in range(1, per_chunk):
         x_copies[i].wait()
         norm_piece(i)
         tok_copy(i).start()
+    for i in range(per_chunk, pieces):
+        x_copies[i].wait()
     w_in[0].wait()
-    w_in[1].wait()
     for copy in smalls + wo_in:
         copy.start(priority=1)
-    for copy in w_in[2:4]:
-        copy.wait()
-    per_chunk = CHUNK // PIECE
+
+    def late_norm():
+        for i in range(per_chunk, pieces):
+            norm_piece(i)
+
+    def late_send():
+        for i in range(per_chunk, pieces):
+            tok_copy(i).start()
 
     def arrive(j):
-        def wait():
-            for i in range(j * per_chunk, (j + 1) * per_chunk):
-                tok_copy(i).wait_recv()
-
-        return wait
+        for i in range(j * per_chunk, (j + 1) * per_chunk):
+            tok_copy(i).wait_recv()
+        if j + 1 == per_half:
+            for copy in w_in[2:] + smalls:
+                copy.wait()
 
     units = own_at + oth_at
     before = None
     for i, unit in enumerate(units):
-        key_unit(unit, functools.partial(state_unit, before) if i > 0 else nothing)
+        key_unit(unit, functools.partial(state_unit, before) if i > 0 else late_norm)
         nxt = i + 1 - per_half
-        value_unit(unit, arrive(nxt) if 0 <= nxt < per_half else nothing)
+        if i == 0:
+            w_in[1].wait()
+            value_unit(unit, late_send)
+        elif 0 <= nxt < per_half:
+            value_unit(unit, functools.partial(arrive, nxt))
+        else:
+            value_unit(unit)
         before = unit
 
     def combine():
@@ -425,70 +437,67 @@
         def _():
             rim_copy.start()
 
-    for copy in w_in[4:] + smalls:
-        copy.wait()
-
     query_unit(units[0], send_rim)
-    query_unit(units[1])
-    query_unit(units[2], functools.partial(relay, 0))
-    query_unit(units[3], functools.partial(relay, 1))
-
-    def mid(unit, c, fence):
-        def run():
-            fence()
-            intra_unit(unit)
-            pool_windows(c)
-
-        return run
-
-    def relays(*cs):
-        def run():
-            for c in cs:
-                relay(c)
-
-        return run
+    query_unit(units[1], functools.partial(relay, 0))
+    query_unit(units[2], functools.partial(relay, 1))
+    query_unit(units[3], functools.partial(relay, 2))
 
     def rim_wait():
-        relay(6)
-        relay(7)
+        for copy in wo_in:
+            copy.wait()
 
         @pl.when(sp > 0)
         def _():
             rim_copy.wait_recv()
 
-    fences = [relays(2), relays(3, 4), relays(5), rim_wait]
+    marks = [(3,), (4, 5), (6, 7)]
     for i, unit in enumerate(units):
         c = (i + 1) % chunks
+
+        def mid():
+            for slot in marks[i] if i < len(marks) else ():
+                relay(slot)
+            if c == 0:
+                rim_wait()
+            intra_unit(unit)
+            pool_windows(c)
+
         score_unit(unit)
-        gate_unit(unit, mid(unit, c, fences[i]))
+        gate_unit(unit, mid)
         pool_mixing(c)
-    for copy in wo_in:
-        copy.wait()
-
-    def pool_share(j):
+    def forward(h, carry):
+        late = (h + HOP * (sp - 1) >= slots) & (sp < n_sp - 1)
+
+        @pl.when(late)
+        def _():
+            st_copy(h).wait_recv()
+            pass_on(h, h)
+            st_copy(h).start()
+
+        return carry
+
+    if n_sp - 2 > slots // HOP:
+        lax.fori_loop(0, heads, forward, 0)
+
+    def last_states():
+        @pl.when((sp > 0) & (sp == n_sp - 1))
+        def _():
+            for h in range(heads):
+                st_copy(h).wait_recv()
+
+    def pool_share(j, between=nothing):
         at = pl.ds(position(oth_at[j]), CHUNK)
         mine = slice(j * CHUNK, (j + 1) * CHUNK)
         for n in range(tiles):
+            if n == tiles - 1:
+                between()
             cols = slice(n * TILE, (n + 1) * TILE)
             acc[mine, cols] = dot(pool_out[at, :], wo[n, :pool_width, :])
 
     for j in range(per_half - 1):
-        pool_share(j)
-    def rest(h, carry):
-        late = (h + HOP * (sp - 1) >= slots) | (sp == n_sp - 1)
-
-        @pl.when(late & (sp > 0))
-        def _():
-            st_copy(h).wait_recv()
-
-            @pl.when(sp < n_sp - 1)
-            def _():
-                pass_on(h, h)
-                st_copy(h).start()
-
-        return carry
-
-    lax.fori_loop(0, heads, rest, 0)
+        pool_share(j, last_states)
+    if per_half == 1:
+        last_states()
 
     def finish(unit):
         start = position(unit)
@@ -503,61 +512,96 @@
             var = jnp.mean(r * r, axis=-1, keepdims=True)
             ret[at, cols] = (gated[at, cols] * (r * lax.rsqrt(var + 1e-06))).astype(BF16)
 
-    def part_copy(j):
+    def part_copy(j, n):
         at = pl.ds(j * CHUNK, CHUNK)
         return pltpu.make_async_remote_copy(
-            src_ref=part_send.at[at],
-            dst_ref=part_recv.at[at],
-            send_sem=part_ss.at[j],
-            recv_sem=part_rs.at[j],
+            src_ref=part_send.at[n, at],
+            dst_ref=part_recv.at[n, at],
+            send_sem=part_ss.at[j, n],
+            recv_sem=part_rs.at[j, n],
             device_id=peer,
             device_id_type=MESH,
         )
 
-    def multiply_other(j, n):
+    def multiply_other(j, n, between=nothing):
         at = pl.ds(position(oth_at[j]), CHUNK)
         mine = slice(j * CHUNK, (j + 1) * CHUNK)
         cols = slice(n * TILE, (n + 1) * TILE)
-        part_send[mine, cols] = (
-            acc[mine, cols] + dot(ret[at, :], wo[n, pool_width:, :])
-        ).astype(BF16)
-
-    def multiply_own(j, n):
+        cut = width // 2
+        res = dot(ret[at, :cut], wo[n, pool_width : pool_width + cut, :])
+        between()
+        res = res + dot(ret[at, cut:], wo[n, pool_width + cut :, :])
+        part_send[n, mine, :] = (acc[mine, cols] + res).astype(BF16)
+
+    def multiply_own(j, n, between=nothing, landed=False):
         at = pl.ds(position(own_at[j]), CHUNK)
         mine = slice(j * CHUNK, (j + 1) * CHUNK)
         cols = slice(n * TILE, (n + 1) * TILE)
-        out_own[mine, cols] = (
-            dot(pool_out[at, :], wo[n, :pool_width, :]) + dot(ret[at, :], wo[n, pool_width:, :])
-        ).astype(BF16)
-
-    def add_received(j):
-        mine = slice(j * CHUNK, (j + 1) * CHUNK)
-        out_own[mine] = (out_own[mine].astype(F32) + part_recv[mine].astype(F32)).astype(BF16)
+        res = dot(pool_out[at, :], wo[n, :pool_width, :])
+        between()
+        res = (res + dot(ret[at, :], wo[n, pool_width:, :])).astype(BF16)
+        if landed:
+            res = (res.astype(F32) + part_recv[n, mine, :].astype(F32)).astype(BF16)
+        out_own[mine, cols] = res
+
+    def add_received(j, n):
+        cols = slice(n * TILE, (n + 1) * TILE)
+        for r in range(j * CHUNK, (j + 1) * CHUNK, 4 * STEP):
+            mine = slice(r, r + 4 * STEP)
+            out_own[mine, cols] = (
+                out_own[mine, cols].astype(F32) + part_recv[n, mine, :].astype(F32)
+            ).astype(BF16)
+
+    def send(j, tiles_of):
+        def start():
+            for n in tiles_of:
+                part_copy(j, n).start()
+
+        return start
+
+    def land(j):
+        def wait():
+            for n in range(tiles):
+                part_copy(j, n).wait_recv()
+
+        return wait
 
     order = oth_at + own_at
+    ready = tiles - 2
     finish(order[0])
     pool_share(per_half - 1)
     for i in range(len(order)):
-        sending = i < per_half
+        j = i % per_half
+        last = i == len(order) - 1
         for n in range(tiles):
-            if n == 1 and 0 < i <= per_half:
-                part_copy(i - 1).start()
-            if n == 1 and i > per_half:
-                part_copy(i - 1 - per_half).wait_recv()
-                add_received(i - 1 - per_half)
-            if n == 2 and i + 1 < len(order):
+            between = nothing
+            if n == 0 and 0 < i < per_half:
+                between = send(i - 1, range(tiles))
+            if n == 0 and i == per_half:
+                between = send(i - 1, range(ready, tiles))
+            if n == tiles - 1 and i == per_half - 1:
+                between = send(i, range(ready))
+            if n == 0 and i > per_half:
+                between = land(j - 1)
+            if n == tiles - 1 and last:
+                between = land(per_half - 1)
+            if i < per_half:
+                multiply_other(j, n, between)
+            else:
+                multiply_own(j, n, between, n == tiles - 1 and last)
+            if n == 0 and not last:
                 finish(order[i + 1])
-            if sending:
-                multiply_other(i, n)
-            else:
-                multiply_own(i - per_half, n)
-    part_copy(per_half - 1).wait_recv()
-    add_received(per_half - 1)
+            if i > per_half and 0 < n < tiles - 1:
+                for k in range(n - 1, tiles, tiles - 2):
+                    add_received(j - 1, k)
+    for n in range(tiles - 1):
+        add_received(per_half - 1, n)
 
     for i in range(pieces):
         tok_copy(i).wait_send()
     for j in range(per_half):
-        part_copy(j).wait_send()
+        for n in range(tiles):
+            part_copy(j, n).wait_send()
 
     @pl.when(sp < n_sp - 1)
     def _():
@@ -636,8 +680,8 @@
             pltpu.VMEM((groups, SUB, SUB + RIM), BF16),
             pltpu.VMEM((heads, 8, HEAD_DIM), F32),
             pltpu.VMEM((rows, wide), F32),
-            pltpu.VMEM((rows, wide), BF16),
-            pltpu.VMEM((rows, wide), BF16),
+            pltpu.VMEM((wide // TILE, rows, TILE), BF16),
+            pltpu.VMEM((wide // TILE, rows, TILE), BF16),
             dma((pieces,)),
             dma((5,)),
             dma((2, wide // TILE)),
@@ -647,8 +691,8 @@
             dma((heads,)),
             dma((heads,)),
             dma((2,)),
-            dma((per_half,)),
-            dma((per_half,)),
+            dma((per_half, wide // TILE)),
+            dma((per_half, wide // TILE)),
         ],
         compiler_params=pltpu.CompilerParams(
             collective_id=0, has_side_effects=True, vmem_limit_bytes=56 * 1024 * 1024

time: 28.6 us -> 27.1 us (0.948)
  Pallas kernels: 27.1 us -> 25.6 us
    pallas_call x1, Pallas kernels: 27.1 us -> 25.6 us  [per_device(): pl.pallas_call(functools.partial(layer_kernel, n_sp, n_tp), out_shape=plt...]
where the time goes in v3:
time: 27.1 us; the launch traced here: 26.9 us
  Pallas kernels  25.6 us (94%)
  local copies, waits for them, and re-layouts  1.32 us (5%)
    pallas_call x1, Pallas kernels, per_device(): pl.pallas_call(functools.partial(layer_kernel, n_sp, n_tp), out_shape=plt...  25.6 us
    unnamed x1, local copies, waits for them, and re-layouts  1.32 us

profile of v3, /device:TPU:31, one launch (start us, length us, event | category | flops | bytes accessed | tf_op | source)
XLA Modules:
  0.0 26.9 jit_solution(10244075495400426424)
XLA Ops:
  0.0 25.6 %shard_map.127 = bf16[512,2048]{1,0:T(8,128)(2,1)S(1)} custom-call(bf16[512,2048]{1,0:T(8,128)(2,1)} %tokens.1, f32[1,2048]{1,0:T(1,128)} %bitcast.3, bf16[2048,512]{1,0:T(8,128)(2,1)} %w_pool.1, bf16[2048,512]{1,0:T(8,128)(2,1)} %w_query.1, bf16[2048,512]{1,0:T(8,128)(2,1)} %w_key.1, bf16[2048,512]{1,0:T(8,128)(2,1)} %w_value.1, bf16[2048,512]{1,0:T(8,128)(2,1)} %w_gate.1, ...), custom_call_target="tpu_custom_call" | custom-call | flops 15032385536 | bytes 20971520 | tf_op jit(solution)/shard_map/pallas_call | solution.py:643
  25.6 1.3 %copy.15 = bf16[512,2048]{1,0:T(8,128)(2,1)} copy(bf16[512,2048]{1,0:T(8,128)(2,1)S(1)} %shard_map.127) | data formatting | bytes 4194304

commit v4 on v3

--- a/solution.py
+++ b/solution.py
@@ -80,6 +80,7 @@
     part_send,
     part_recv,
     x_sem,
+    key_sem,
     w_sem,
     wo_sem,
     small_sem,
@@ -117,9 +118,16 @@
         at = pl.ds(i * PIECE, PIECE)
         x_copies.append(pltpu.make_async_copy(tokens.at[at], x_in.at[at], x_sem.at[i]))
         x_copies[i].start()
-    w_in = [
-        pltpu.make_async_copy(w, wts.at[i], w_sem.at[i])
-        for i, w in enumerate((w_key, w_value, w_pool, w_query, w_gate))
+    deep = w_key.shape[0] // 2
+    key_in = [
+        pltpu.make_async_copy(
+            w_key.at[pl.ds(i * deep, deep)], wts.at[0, pl.ds(i * deep, deep)], key_sem.at[i]
+        )
+        for i in range(2)
+    ]
+    w_in = key_in[:1] + [
+        pltpu.make_async_copy(w, wts.at[i + 1], w_sem.at[i])
+        for i, w in enumerate((w_value, w_pool, w_query, w_gate))
     ]
     smalls = [
         pltpu.make_async_copy(src, dst, small_sem.at[i + 1])
@@ -136,7 +144,7 @@
         for i, (src, low) in enumerate(((w_out_pool, 0), (w_out_ret, pool_width)))
         for n in range(tiles)
     ]
-    for copy in w_in:
+    for copy in key_in + w_in[1:]:
         copy.start(priority=1)
 
     barrier = pltpu.get_barrier_semaphore()
@@ -232,24 +240,27 @@
     own_at = [(tok_own, own, j) for j in range(per_half)]
     oth_at = [(tok_oth, other, j) for j in range(per_half)]
 
+    def span_of(unit):
+        return unit[3] if len(unit) > 3 else CHUNK
+
     def position(unit):
         return pl.multiple_of(unit[1] + unit[2] * CHUNK, CHUNK)
 
     def project(w, unit, lo=0, hi=blocks, res=None):
-        src, _, j = unit
-        mine = slice(j * CHUNK, (j + 1) * CHUNK)
+        src, _, j = unit[:3]
+        mine = slice(j * CHUNK, j * CHUNK + span_of(unit))
         for n in range(lo, hi):
             term = dot(src[n, mine, :], wts[w, n * TILE : (n + 1) * TILE, :])
             res = term if res is None else res + term
         return res
 
+    def nothing():
+        pass
+
     def split(w, unit, between):
         res = project(w, unit, 0, half)
         between()
         return project(w, unit, half, blocks, res)
-
-    def nothing():
-        pass
 
     def head_cols(h):
         return slice(h * HEAD_DIM, (h + 1) * HEAD_DIM)
@@ -277,11 +288,11 @@
             )
 
     def pool_unit(unit, between=nothing):
-        at = pl.ds(pl.multiple_of(position(unit) + RIM, RIM), CHUNK)
+        at = pl.ds(pl.multiple_of(position(unit) + RIM, RIM), span_of(unit))
         pp[at] = split(2, unit, between).astype(BF16)
 
     def query_unit(unit, between=nothing):
-        at = pl.ds(position(unit), CHUNK)
+        at = pl.ds(position(unit), span_of(unit))
         q = split(3, unit, between)
         for h in range(heads):
             qr[at, head_cols(h)] = rotate(q[:, head_cols(h)].astype(BF16).astype(F32), at).astype(BF16)
@@ -377,11 +388,12 @@
         tok_copy(i).start()
     for i in range(per_chunk, pieces):
         x_copies[i].wait()
-    w_in[0].wait()
+    key_in[0].wait()
     for copy in smalls + wo_in:
         copy.start(priority=1)
 
     def late_norm():
+        key_in[1].wait()
         for i in range(per_chunk, pieces):
             norm_piece(i)
 
@@ -429,8 +441,9 @@
         for h in range(heads):
             st_copy(h).start()
 
-    for unit in units[1:]:
+    for unit in units[1:per_half]:
         pool_unit(unit)
+    pool_unit((tok_oth, other, 0, rows))
 
     def send_rim():
         @pl.when(sp < n_sp - 1)
@@ -489,15 +502,10 @@
         at = pl.ds(position(oth_at[j]), CHUNK)
         mine = slice(j * CHUNK, (j + 1) * CHUNK)
         for n in range(tiles):
-            if n == tiles - 1:
+            if n == 1:
                 between()
             cols = slice(n * TILE, (n + 1) * TILE)
             acc[mine, cols] = dot(pool_out[at, :], wo[n, :pool_width, :])
-
-    for j in range(per_half - 1):
-        pool_share(j, last_states)
-    if per_half == 1:
-        last_states()
 
     def finish(unit):
         start = position(unit)
@@ -568,8 +576,13 @@
 
     order = oth_at + own_at
     ready = tiles - 2
-    finish(order[0])
-    pool_share(per_half - 1)
+
+    def begin():
+        last_states()
+        finish(order[0])
+
+    for k in range(per_half):
+        pool_share(k, begin if k == per_half - 1 else nothing)
     for i in range(len(order)):
         j = i % per_half
         last = i == len(order) - 1
@@ -683,7 +696,8 @@
             pltpu.VMEM((wide // TILE, rows, TILE), BF16),
             pltpu.VMEM((wide // TILE, rows, TILE), BF16),
             dma((pieces,)),
-            dma((5,)),
+            dma((2,)),
+            dma((4,)),
             dma((2, wide // TILE)),
             dma((5,)),
             dma((pieces,)),

time: 27.1 us -> 27 us (level)
  the two profiles are of different devices: /device:TPU:31 before, /device:TPU:0 now
where the time goes in v4:
time: 27 us; the launch traced here: 26.8 us
  Pallas kernels  25.5 us (94%)
  local copies, waits for them, and re-layouts  1.32 us (5%)
    pallas_call x1, Pallas kernels, per_device(): pl.pallas_call(functools.partial(layer_kernel, n_sp, n_tp), out_shape=plt...  25.5 us
    unnamed x1, local copies, waits for them, and re-layouts  1.32 us

profile of v4, /device:TPU:0, one launch (start us, length us, event | category | flops | bytes accessed | tf_op | source)
XLA Modules:
  0.0 26.8 jit_solution(795608886498927078)
XLA Ops:
  0.0 25.5 %shard_map.127 = bf16[512,2048]{1,0:T(8,128)(2,1)S(1)} custom-call(bf16[512,2048]{1,0:T(8,128)(2,1)} %tokens.1, f32[1,2048]{1,0:T(1,128)} %bitcast.3, bf16[2048,512]{1,0:T(8,128)(2,1)} %w_pool.1, bf16[2048,512]{1,0:T(8,128)(2,1)} %w_query.1, bf16[2048,512]{1,0:T(8,128)(2,1)} %w_key.1, bf16[2048,512]{1,0:T(8,128)(2,1)} %w_value.1, bf16[2048,512]{1,0:T(8,128)(2,1)} %w_gate.1, ...), custom_call_target="tpu_custom_call" | custom-call | flops 15032385536 | bytes 20971520 | tf_op jit(solution)/shard_map/pallas_call | solution.py:656
  25.5 1.3 %copy.15 = bf16[512,2048]{1,0:T(8,128)(2,1)} copy(bf16[512,2048]{1,0:T(8,128)(2,1)S(1)} %shard_map.127) | data formatting | bytes 4194304
